TPU v7x, 32 devices: a whole 2x2x4 slice. The times are simulated.
32 devices in a mesh: ep: 8 (over z, y), tp: 4 (over x, core).
Axes of the slice: x: 2, y: 2, z: 4, core: 2. Of those that a mesh axis runs over, the one named last changes fastest.
Arguments:
- query_rows: bfloat16 [8192, 1024], P('ep', 'tp'), may hold values from -140 to 140
- key_rows: bfloat16 [8192, 256], P('ep', 'tp'), may hold values from -4.5 to 4.5
- value_rows: bfloat16 [8192, 256], P('ep', 'tp'), may hold values from -6 to 6
- sink_logit: float32 [16], P('tp'), may hold values from 1 to 6
- out_weight: bfloat16 [1024, 2048], P('tp'), may hold values from -0.1875 to 0.1875
- routed_rows: bfloat16 [4096, 2048], P(('ep', 'tp')), may hold values from -6 to 6
- norm_gain: float32 [2048], replicated, may hold values from 0.1 to 1.9
- routing: int32 [4096, 2], P(('ep', 'tp')), may hold values from 0 to 7, all different within a row; in each aligned block of 128 rows (0 to 127, 128 to 255, ...) at most 36 rows name the same one
- route_weight: float32 [4096, 2], P(('ep', 'tp')), may hold values from 0.2 to 1
- gate_weight: bfloat16 [8, 2048, 7168], P('ep', None, 'tp'), may hold values from -0.125 to 0.125
- up_weight: bfloat16 [8, 2048, 7168], P('ep', None, 'tp'), may hold values from -0.125 to 0.125
- down_weight: bfloat16 [8, 7168, 2048], P('ep', 'tp'), may hold values from -0.0625 to 0.0625
Outputs:
- mixed_rows: bfloat16 [8192, 2048], P(('ep', 'tp'))
- expert_mix: bfloat16 [4096, 2048], P(('ep', 'tp'))
Inputs may be any that keep to these rules, and one draw needn't show every extreme that they name: `routing`: each token names 2 different experts. Within the 128 rows of one device no expert is named by more than 36 rows, and in every draw some device's rows name some expert exactly 36 times.
All inputs are finite; a program needn't handle non-finite values.
Results may differ from a plain program's by a relative error of at most 0.012.
Values may be sent and summed in bfloat16 or wider, within the bound.
A program may use at most 128 MiB of HBM per device.

v0:
```python
import jax
import jax.numpy as jnp
from jax import lax
from jax.sharding import PartitionSpec as P

HEAD_DIM = 64
WINDOW = 128
EPS = 1e-06


def padded_2(value, sides, width):
    for axis, dim in sides:
        peers, length = (lax.axis_size(axis), value.shape[dim])
        up = [(i, (i + 1) % peers) for i in range(peers - 1)]
        down = [(j, i) for i, j in up]
        last = lax.slice_in_dim(value, length - width, length, axis=dim)
        leading = lax.slice_in_dim(value, 0, width, axis=dim)
        before = lax.ppermute(last, axis, up)
        after = lax.ppermute(leading, axis, down)
        value = jnp.concatenate([before, value, after], axis=dim)
    return value


def expert_hidden(arrived, gate_weight, up_weight):
    gate_pre = jnp.einsum(
        "scd,df->scf", arrived, gate_weight[0], preferred_element_type=jnp.float32
    )
    up_pre = jnp.einsum("scd,df->scf", arrived, up_weight[0], preferred_element_type=jnp.float32)
    return (jax.nn.silu(gate_pre) * up_pre).astype(jnp.bfloat16)


def window_attention(query_rows, key_rows, value_rows, sink_logit):
    row_count = query_rows.shape[0]
    kv_here = key_rows.shape[1] // HEAD_DIM
    group_size = query_rows.shape[1] // (kv_here * HEAD_DIM)
    block_rows = min(512, row_count)
    joined = jnp.concatenate([key_rows, value_rows], axis=1)
    padded = padded_2(joined, (("ep", 0),), WINDOW)
    seq_total = row_count * lax.axis_size("ep")
    offset = lax.axis_index("ep") * row_count
    sink_col = sink_logit.reshape(kv_here, group_size)[:, :, None]
    score_scale = HEAD_DIM ** (-0.5)

    def one_block(block_index):
        first_row = block_index * block_rows
        query_block = lax.dynamic_slice_in_dim(query_rows, first_row, block_rows, 0).reshape(
            block_rows, kv_here, group_size, HEAD_DIM
        )
        key_span = lax.dynamic_slice_in_dim(padded, first_row, block_rows + 2 * WINDOW, 0)
        key_block = key_span[:, : kv_here * HEAD_DIM].reshape(-1, kv_here, HEAD_DIM)
        value_block = key_span[:, kv_here * HEAD_DIM :].reshape(-1, kv_here, HEAD_DIM)
        scores = (
            jnp.einsum("qkgd,skd->kgqs", query_block, key_block, preferred_element_type=jnp.float32)
            * score_scale
        )
        query_pos = first_row + jnp.arange(block_rows, dtype=jnp.int32)
        key_pos = first_row - WINDOW + jnp.arange(block_rows + 2 * WINDOW, dtype=jnp.int32)
        global_pos = offset + key_pos
        inside = (
            (jnp.abs(key_pos[None, :] - query_pos[:, None]) <= WINDOW)
            & (global_pos >= 0)[None, :]
            & (global_pos < seq_total)[None, :]
        )
        scores = jnp.where(inside, scores, -jnp.inf)
        row_peak = jnp.maximum(jnp.max(scores, axis=-1), sink_col)
        weights = jnp.exp(scores - row_peak[..., None])
        total_weight = jnp.sum(weights, axis=-1) + jnp.exp(sink_col - row_peak)
        attended = jnp.einsum(
            "kgqs,skd->qkgd",
            weights.astype(jnp.bfloat16),
            value_block,
            preferred_element_type=jnp.float32,
        )
        attended = attended / jnp.transpose(total_weight, (2, 0, 1))[..., None]
        return attended.reshape(block_rows, -1).astype(jnp.bfloat16)

    pieces = lax.map(one_block, jnp.arange(row_count // block_rows, dtype=jnp.int32))
    return pieces.reshape(row_count, -1)


def body(
    query_rows,
    key_rows,
    value_rows,
    sink_logit,
    out_weight,
    routed_rows,
    norm_gain,
    routing,
    route_weight,
    gate_weight,
    up_weight,
    down_weight,
):
    attended = window_attention(query_rows, key_rows, value_rows, sink_logit)
    projected = lax.psum_scatter(
        jnp.dot(attended, out_weight, preferred_element_type=jnp.float32).astype(jnp.bfloat16),
        "tp",
        scatter_dimension=0,
        tiled=True,
    )
    token_count, model_width = routed_rows.shape
    top_count = routing.shape[1]
    experts = lax.axis_size("ep")
    capacity = token_count * top_count * 9 // (8 * experts)
    values = routed_rows.astype(jnp.float32)
    normed = (
        values * lax.rsqrt(jnp.mean(values * values, axis=-1, keepdims=True) + EPS) * norm_gain
    ).astype(jnp.bfloat16)
    chosen = routing.reshape(-1)
    onehot = (chosen[:, None] == jnp.arange(experts, dtype=jnp.int32)[None, :]).astype(jnp.int32)
    before = jnp.cumsum(onehot, axis=0) - onehot
    slot_index = jnp.sum(before * onehot, axis=1)
    target = chosen * capacity + slot_index
    outgoing = (
        jnp.zeros((experts * capacity, model_width), jnp.bfloat16)
        .at[target]
        .set(jnp.repeat(normed, top_count, axis=0))
    )
    outgoing = outgoing.reshape(experts, capacity, model_width)
    hidden = expert_hidden(
        lax.all_gather(
            lax.all_to_all(outgoing, "ep", split_axis=0, concat_axis=0, tiled=True),
            "tp",
            axis=0,
            tiled=True,
        ),
        gate_weight,
        up_weight,
    )
    rounded = jnp.einsum(
        "scf,fd->scd", hidden, down_weight[0], preferred_element_type=jnp.float32
    ).astype(jnp.bfloat16)
    summed = lax.psum_scatter(
        lax.optimization_barrier(rounded).astype(jnp.float32).astype(jnp.bfloat16),
        "tp",
        scatter_dimension=0,
        tiled=True,
    ).astype(jnp.float32)
    results = lax.all_to_all(
        summed.astype(jnp.bfloat16), "ep", split_axis=0, concat_axis=0, tiled=True
    ).astype(summed.dtype)
    slot_results = results.reshape(experts * capacity, model_width)
    picked = slot_results[target] * route_weight.reshape(-1)[:, None]
    expert_mix = jnp.sum(picked.reshape(token_count, top_count, model_width), axis=1).astype(
        jnp.bfloat16
    )
    return (projected, expert_mix)


def solution(mesh):
    in_specs = (
        P("ep", "tp"),
        P("ep", "tp"),
        P("ep", "tp"),
        P("tp"),
        P("tp", None),
        P(("ep", "tp"), None),
        P(),
        P(("ep", "tp"), None),
        P(("ep", "tp"), None),
        P("ep", None, "tp"),
        P("ep", None, "tp"),
        P("ep", "tp", None),
    )
    out_specs = (P(("ep", "tp"), None), P(("ep", "tp"), None))
    return jax.shard_map(body, mesh=mesh, in_specs=in_specs, out_specs=out_specs, check_vma=False)
```

profile of v0, /device:TPU:0, one launch (start us, length us, event | category | flops | bytes accessed | tf_op | source)
XLA Modules:
  0.0 254.0 jit_solution(6978425806556693117)
XLA Ops:
  7.2 0.9 copy.28
  10.1 1.2 fusion.47
  11.4 1.2 fusion.49
  13.3 1.2 reshape.293
  14.6 3.1 %scatter_custom_fusion = bf16[288,2048]{1,0:T(8,128)(2,1)S(1)} fusion(s32[256]{0:T(256)S(1)} %bitcast.135, bf16[256,2048]{1,0:T(8,128)(2,1)} %reshape.293, bf16[]{:T(256)} %constant.85.clone.1), kind=kCustom, calls=%fused_computation.52 | custom fusion | bytes 1180160 | tf_op jit(solution)/shard_map/scatter | solution.py:118
  18.0 38.5 %all_to_all.10 = bf16[8,36,2048]{2,1,0:T(8,128)(2,1)S(1)} all-to-all(bf16[8,36,2048]{2,1,0:T(8,128)(2,1)S(1)} %reshape.276), channel_id=1, replica_groups=mesh['ep'=8,'tp'=4] {'ep'}, dimensions={0} | all-to-all | bytes 2359296 | tf_op jit(solution)/shard_map/all_to_all | solution.py:123
  56.5 1.7 copy.30
  58.2 36.5 %all-gather.2.cloned.1.call-done = bf16[32,36,2048]{2,0,1:T(8,128)(2,1)} async-done(((bf16[8,36,2048]{2,0,1:T(8,128)(2,1)}), bf16[32,36,2048]{2,0,1:T(8,128)(2,1)}) %all-gather.2.cloned.1.call-update) | async-done | bytes 4718608 | tf_op jit(solution)/shard_map/all_gather | solution.py:122
  94.8 19.5 %fusion.28 = f32[32,36,1792]{2,1,0:T(8,128)} fusion(bf16[1,2048,1792]{2,1,0:T(8,128)(2,1)} %param.24, bf16[32,36,2048]{2,0,1:T(8,128)(2,1)} %all-gather.2.cloned.1.call-done), kind=kOutput, calls=%fused_computation.37 | convolution fusion | flops 8455716864 | bytes 20316160 | tf_op jit(solution)/shard_map/scd,df->scf/dot_general | solution.py:28
  114.3 33.8 %fusion.40 = bf16[32,36,2048]{2,1,0:T(8,128)(2,1)} fusion(bf16[1,1792,2048]{2,1,0:T(8,128)(2,1)} %param.25, f32[32,36,1792]{2,1,0:T(8,128)} %fusion.28, bf16[1,2048,1792]{2,1,0:T(8,128)(2,1)} %param.23, bf16[32,36,2048]{2,0,1:T(8,128)(2,1)} %all-gather.2.cloned.1.call-done), kind=kOutput, calls=%fused_computation.44 | convolution fusion | flops 16926179328 | bytes 32374784 | tf_op jit(solution)/shard_map/scf,fd->scd/dot_general | solution.py:131
  148.2 3.5 %collective-permute-start = (bf16[128,128]{0,1:T(8,128)(2,1)S(1)}, bf16[128,128]{0,1:T(8,128)(2,1)S(1)}, u32[]{:S(2)}, u32[]{:S(2)}) collective-permute-start(bf16[128,128]{0,1:T(8,128)(2,1)S(1)} %get-tuple-element.131), channel_id=1, source_target_pairs={{0,4},{4,8},{8,12},{12,16},{16,20},{20,24},{24,28},{1,5},{5,9},{9,... | collective-permute-start | bytes 98312 | tf_op jit(solution)/shard_map/ppermute | solution.py:18
  151.8 1.3 collective-permute-start.1
  153.3 4.2 %collective-permute-done.1 = bf16[128,128]{0,1:T(8,128)(2,1)S(1)} collective-permute-done((bf16[128,128]{0,1:T(8,128)(2,1)S(1)}, bf16[128,128]{0,1:T(8,128)(2,1)S(1)}, u32[]{:S(2)}, u32[]{:S(2)}) %collective-permute-start.1) | collective-permute-done | bytes 32800 | tf_op jit(solution)/shard_map/ppermute | solution.py:19
  157.6 25.5 %while.12 = (s32[]{:T(128)}, bf16[2,512,256]{2,1,0:T(8,128)(2,1)S(1)}, s32[2]{0:T(128)S(1)}, bf16[1280,128]{0,1:T(8,128)(2,1)S(1)}, s32[]{:T(128)}, /*index=5*/b...) while((s32[]{:T(128)}, ...), condition=%wide.region_3.4_spmd, body=%wide.region_0.3_spmd.sunk | while | flops 422191360 | bytes 48526672 | solution.py:77
  159.2 0.8 fusion.69
  160.2 1.2 fusion.70
  161.5 2.6 %copy-done.1 = f32[768,512,4]{1,0,2:T(8,128)} copy-done((f32[768,512,4]{1,0,2:T(8,128)}, f32[768,512,4]{1,0,2:T(8,128)S(1)}, u32[]{:S(2)}) %copy-start.1) | copy-done | bytes 6291480 | tf_op jit(solution)/shard_map/while
  164.1 1.4 fusion.71
  165.5 5.0 %fusion.73 = bf16[512,1,4,64]{0,3,2,1:T(8,128)(2,1)S(1)} fusion(f32[768,512,4]{1,0,2:T(8,128)} %copy-done.1, f32[4,512]{1,0:T(4,128)S(1)} %broadcast_maximum_fusion.2, pred[512,768]{0,1:T(8,128)(4,1)S(1)} %fusion.69, f32[512,4]{0,1:T(4,128)S(1)} %fusion.72, bf16[1280,128]{0,1:T(8,128)(2,1)S(1)} %get-tuple-element.215, s32[]{:T(128)S(6)} %select_n.57, ...), kind=kOutput, calls=%fused_computation.15.clone.1 | convolution fusion | flops 207880192 | bytes 7061512 | tf_op jit(solution)/shard_map/while/body/eval_jaxpr/kgqs,skd->qkgd/dot_general | solution.py:68
  172.1 0.8 fusion.69
  173.1 1.2 fusion.70
  174.4 2.6 %copy-done.1 = f32[768,512,4]{1,0,2:T(8,128)} copy-done((f32[768,512,4]{1,0,2:T(8,128)}, f32[768,512,4]{1,0,2:T(8,128)S(1)}, u32[]{:S(2)}) %copy-start.1) | copy-done | bytes 6291480 | tf_op jit(solution)/shard_map/while
  176.9 1.4 fusion.71
  178.4 4.6 %fusion.73 = bf16[512,1,4,64]{0,3,2,1:T(8,128)(2,1)S(1)} fusion(f32[768,512,4]{1,0,2:T(8,128)} %copy-done.1, f32[4,512]{1,0:T(4,128)S(1)} %broadcast_maximum_fusion.2, pred[512,768]{0,1:T(8,128)(4,1)S(1)} %fusion.69, f32[512,4]{0,1:T(4,128)S(1)} %fusion.72, bf16[1280,128]{0,1:T(8,128)(2,1)S(1)} %get-tuple-element.215, s32[]{:T(128)S(6)} %select_n.57, ...), kind=kOutput, calls=%fused_computation.15.clone.1 | convolution fusion | flops 207880192 | bytes 7061512 | tf_op jit(solution)/shard_map/while/body/eval_jaxpr/kgqs,skd->qkgd/dot_general | solution.py:68
  183.2 3.2 %convolution_convert_fusion = bf16[1024,2048]{1,0:T(8,128)(2,1)} fusion(bf16[1024,256]{1,0:T(8,128)(2,1)S(1)} %bitcast.131, bf16[256,2048]{1,0:T(8,128)(2,1)S(1)} %copy-done), kind=kOutput, calls=%fused_computation.45 | convolution fusion | flops 1075838976 | bytes 5767168 | tf_op jit(solution)/shard_map/dot_general | solution.py:97
  186.4 13.3 %reduce-scatter.5.cloned.1.call-done = bf16[8,36,2048]{2,1,0:T(8,128)(2,1)} async-done(((bf16[32,36,2048]{2,1,0:T(8,128)(2,1)}), bf16[8,36,2048]{2,1,0:T(8,128)(2,1)}) %reduce-scatter.5.cloned.1.call-update) | async-done | bytes 1179664 | tf_op jit(solution)/shard_map/reduce_scatter | solution.py:134
  199.6 5.5 %all-to-all-start.1 = ((bf16[8,36,2048]{2,1,0:T(8,128)(2,1)}), bf16[8,36,2048]{2,1,0:T(8,128)(2,1)}, u32[]{:S(2)}, u32[]{:S(2)}) async-start(bf16[8,36,2048]{2,1,0:T(8,128)(2,1)} %reduce-scatter.5.cloned.1.call-done), calls=%async_computation.3 | async-start | bytes 2621440 | tf_op jit(solution)/shard_map/all_to_all | solution.py:140
  205.3 31.2 %all-to-all-done.1 = bf16[8,36,2048]{2,1,0:T(8,128)(2,1)} async-done(((bf16[8,36,2048]{2,1,0:T(8,128)(2,1)}), bf16[8,36,2048]{2,1,0:T(8,128)(2,1)}, u32[]{:S(2)}, u32[]{:S(2)}) %all-to-all-start.1) | async-done | bytes 1179680 | tf_op jit(solution)/shard_map/all_to_all | solution.py:140
  236.5 1.4 reshape.280
  237.9 2.7 %gather_fusion = f32[256,2048]{1,0:T(8,128)} fusion(f32[288,2048]{1,0:T(8,128)S(1)} %reshape.280, s32[1024]{0:T(1024)S(1)} %pad_clamp_fusion), kind=kCustom, calls=%fused_computation | custom fusion | bytes 4195328 | tf_op jit(solution)/shard_map/gather | solution.py:144
  240.6 2.5 gather.6
  243.1 3.9 %multiply_reduce_fusion = bf16[128,2048]{1,0:T(8,128)(2,1)} fusion(f32[128,2,2048]{2,1,0:T(2,128)S(1)} %gather.6, f32[128,2]{1,0:T(8,128)S(1)} %copy.33), kind=kLoop, calls=%fused_computation.46 | loop fusion | flops 786432 | bytes 2622464 | tf_op jit(solution)/shard_map/reduce_sum | solution.py:145
  (65 shorter events, 6.5 us)
Async XLA Ops:
  7.2 176.0 %copy-start = (bf16[256,2048]{1,0:T(8,128)(2,1)S(1)}, bf16[256,2048]{1,0:T(8,128)(2,1)}, u32[]{:S(2)}) copy-start(bf16[256,2048]{1,0:T(8,128)(2,1)} %param.18) | copy-start | bytes 3145732
  7.2 87.6 %all-gather.2.cloned.1.call-start = ((), (), s32[]{:S(2)}) async-start(), calls=%async_computation.5 | async-start | bytes 5898240 | tf_op jit(solution)/shard_map/all_gather | solution.py:122
  58.2 141.4 %reduce-scatter.5.cloned.1.call-start = ((), (), s32[]{:S(2)}) async-start(), calls=%async_computation.6 | async-start | bytes 6553600 | tf_op jit(solution)/shard_map/reduce_scatter | solution.py:134
  114.3 33.9 %copy-start.3 = (bf16[1024,64]{0,1:T(8,128)(2,1)S(1)}, bf16[1024,64]{0,1:T(8,128)(2,1)}, u32[]{:S(2)}) copy-start(bf16[1024,64]{0,1:T(8,128)(2,1)} %param.15) | copy-start | bytes 393220
  114.3 33.9 %copy-start.4 = (bf16[1024,64]{0,1:T(8,128)(2,1)S(1)}, bf16[1024,64]{0,1:T(8,128)(2,1)}, u32[]{:S(2)}) copy-start(bf16[1024,64]{0,1:T(8,128)(2,1)} %param.16) | copy-start | bytes 393220
  148.1 9.5 %copy-start.2 = (bf16[1024,256]{1,0:T(8,128)(2,1)S(1)}, bf16[1024,256]{1,0:T(8,128)(2,1)}, u32[]{:S(2)}) copy-start(bf16[1024,256]{1,0:T(8,128)(2,1)} %param.14) | copy-start | bytes 1572868
  148.1 9.5 %copy-start.5 = (f32[4]{0:T(128)S(1)}, f32[4]{0:T(128)}, u32[]{:S(2)}) copy-start(f32[4]{0:T(128)} %param.17) | copy-start | bytes 52
  148.1 99.3 %reduce-scatter.3.cloned.1.call-start = ((), (), s32[]{:S(2)}) async-start(), calls=%async_computation.4 | async-start | bytes 5242880 | tf_op jit(solution)/shard_map/reduce_scatter | solution.py:96
  148.2 5.1 %collective-permute-start = (bf16[128,128]{0,1:T(8,128)(2,1)S(1)}, bf16[128,128]{0,1:T(8,128)(2,1)S(1)}, u32[]{:S(2)}, u32[]{:S(2)}) collective-permute-start(bf16[128,128]{0,1:T(8,128)(2,1)S(1)} %get-tuple-element.131), channel_id=1, source_target_pairs={{0,4},{4,8},{8,12},{12,16},{16,20},{20,24},{24,28},{1,5},{5,9},{9,... | collective-permute-start | bytes 98312 | tf_op jit(solution)/shard_map/ppermute | solution.py:18
  151.8 5.8 %collective-permute-start.1 = (bf16[128,128]{0,1:T(8,128)(2,1)S(1)}, bf16[128,128]{0,1:T(8,128)(2,1)S(1)}, u32[]{:S(2)}, u32[]{:S(2)}) collective-permute-start(bf16[128,128]{0,1:T(8,128)(2,1)S(1)} %get-tuple-element.132), channel_id=1, source_target_pairs={{4,0},{8,4},{12,8},{16,12},{20,16},{24,20},{28,24},{5,1},{9,5},{13... | collective-permute-start | bytes 98312 | tf_op jit(solution)/shard_map/ppermute | solution.py:19
  161.4 2.7 %copy-start.1 = (f32[768,512,4]{1,0,2:T(8,128)}, f32[768,512,4]{1,0,2:T(8,128)S(1)}, u32[]{:S(2)}) copy-start(f32[768,512,4]{1,0,2:T(8,128)S(1)} %get-tuple-element.182) | copy-start | bytes 18874372 | tf_op jit(solution)/shard_map/while
  174.3 2.7 %copy-start.1 = (f32[768,512,4]{1,0,2:T(8,128)}, f32[768,512,4]{1,0,2:T(8,128)S(1)}, u32[]{:S(2)}) copy-start(f32[768,512,4]{1,0,2:T(8,128)S(1)} %get-tuple-element.182) | copy-start | bytes 18874372 | tf_op jit(solution)/shard_map/while
  183.1 22.0 %copy-start.6 = (f32[128,2]{0,1:T(2,128)S(1)}, f32[128,2]{0,1:T(2,128)}, u32[]{:S(2)}) copy-start(f32[128,2]{0,1:T(2,128)} %param.22) | copy-start | bytes 3076
  199.6 36.8 %all-to-all-start.1 = ((bf16[8,36,2048]{2,1,0:T(8,128)(2,1)}), bf16[8,36,2048]{2,1,0:T(8,128)(2,1)}, u32[]{:S(2)}, u32[]{:S(2)}) async-start(bf16[8,36,2048]{2,1,0:T(8,128)(2,1)} %reduce-scatter.5.cloned.1.call-done), calls=%async_computation.3 | async-start | bytes 2621440 | tf_op jit(solution)/shard_map/all_to_all | solution.py:140
Sparse Core Ops, SparseCore 0:
  58.3 36.4 all-gather.1
  148.2 51.3 reduce-scatter.4
  202.7 44.6 reduce-scatter.2
where the time goes:
time: 254 us
  waiting for transfers between devices  86 us (34%)
  matrix products  68.4 us (27%)
  blocking collectives  38.5 us (15%)
  local copies, waits for them, and re-layouts  22.4 us (9%)
  between operations  13.9 us (5%)
  other arithmetic  12.5 us (5%)
  starting transfers between devices  10.4 us (4%)
    all_to_all x1, blocking collectives, body(): lax.all_to_all(outgoing, 'ep', split_axis=0, concat_axis=0, tiled=True)  38.5 us
    all_gather x1, waiting for transfers between devices, body(): lax.all_gather(lax.all_to_all(outgoing, 'ep', split_axis=0, concat_axis=0...  36.5 us
    dot_general x1, matrix products, body(): jnp.einsum('scf,fd->scd', hidden, down_weight[0], preferred_element_type=...  33.8 us
    all_to_all x1, waiting for transfers between devices, body(): lax.all_to_all(summed.astype(jnp.bfloat16), 'ep', split_axis=0, concat_ax...  31.2 us
    dot_general x1, matrix products, expert_hidden(): jnp.einsum('scd,df->scf', arrived, up_weight[0], preferred_element_type=j...  19.5 us
    reduce_scatter x1, waiting for transfers between devices, body(): lax.psum_scatter(lax.optimization_barrier(rounded).astype(jnp.float32).as...  13.3 us
    dot_general x2, matrix products, one_block(): jnp.einsum('kgqs,skd->qkgd', weights.astype(jnp.bfloat16), value_block, p...  9.53 us
    all_to_all x1, starting transfers between devices, body(): lax.all_to_all(summed.astype(jnp.bfloat16), 'ep', split_axis=0, concat_ax...  5.52 us
  transfers between devices with their start and end apart: 6, of which 6 were waited for; matrix products, arithmetic and copies ran while one was open for 13% of the time, Pallas kernels for 0%

commit v1 on v0

--- a/solution.py
+++ b/solution.py
@@ -6,6 +6,12 @@
 HEAD_DIM = 64
 WINDOW = 128
 EPS = 1e-06
+
+
+def gather_by_exchange(x, axis, dim):
+    count = lax.axis_size(axis)
+    repeats = [count if d == dim else 1 for d in range(x.ndim)]
+    return lax.all_to_all(jnp.tile(x, repeats), axis, split_axis=dim, concat_axis=dim, tiled=True)
 
 
 def padded_2(value, sides, width):
@@ -119,11 +125,8 @@
     )
     outgoing = outgoing.reshape(experts, capacity, model_width)
     hidden = expert_hidden(
-        lax.all_gather(
-            lax.all_to_all(outgoing, "ep", split_axis=0, concat_axis=0, tiled=True),
-            "tp",
-            axis=0,
-            tiled=True,
+        gather_by_exchange(
+            lax.all_to_all(outgoing, "ep", split_axis=0, concat_axis=0, tiled=True), "tp", 0
         ),
         gate_weight,
         up_weight,

time: 254 us -> 269 us (1.059)
  blocking collectives: 38.5 us -> 101 us
  waiting for transfers between devices: 86 us -> 47.2 us
  matrix products: 68.4 us -> 58.4 us
    all_to_all x0 -> x1, blocking collectives: none -> 62.2 us  [gather_by_exchange(): lax.all_to_all(jnp.tile(x, repeats), axis, split_axis=dim, concat_axis=di...]
    all_gather x1 -> x0, waiting for transfers between devices: 36.5 us -> none  [body(): lax.all_gather(lax.all_to_all(outgoing, 'ep', split_axis=0, concat_axis=0...]
    dot_general x1, matrix products: 19.5 us -> 12.1 us  [expert_hidden(): jnp.einsum('scd,df->scf', arrived, up_weight[0], preferred_element_type=j...]
    dot_general x1, matrix products: 33.8 us -> 30.9 us  [body(): jnp.einsum('scf,fd->scd', hidden, down_weight[0], preferred_element_type=...]
  transfers between devices with their start and end apart: 6 -> 5, of which waited for: 6 -> 4; matrix products, arithmetic and copies ran while one was open for 13% -> 12% of each run, Pallas kernels for 0% -> 0%
where the time goes in v1:
time: 269 us
  blocking collectives  101 us (38%)
  matrix products  58.4 us (22%)
  waiting for transfers between devices  47.2 us (18%)
  local copies, waits for them, and re-layouts  23.7 us (9%)
  between operations  14.3 us (5%)
  other arithmetic  12.5 us (5%)
  starting transfers between devices  10.6 us (4%)
    all_to_all x1, blocking collectives, gather_by_exchange(): lax.all_to_all(jnp.tile(x, repeats), axis, split_axis=dim, concat_axis=di...  62.2 us
    all_to_all x1, blocking collectives, body(): lax.all_to_all(outgoing, 'ep', split_axis=0, concat_axis=0, tiled=True)  38.5 us
    all_to_all x1, waiting for transfers between devices, body(): lax.all_to_all(summed.astype(jnp.bfloat16), 'ep', split_axis=0, concat_ax...  31.2 us
    dot_general x1, matrix products, body(): jnp.einsum('scf,fd->scd', hidden, down_weight[0], preferred_element_type=...  30.9 us
    dot_general x1, matrix products, expert_hidden(): jnp.einsum('scd,df->scf', arrived, up_weight[0], preferred_element_type=j...  12.1 us
    reduce_scatter x1, waiting for transfers between devices, body(): lax.psum_scatter(lax.optimization_barrier(rounded).astype(jnp.float32).as...  11.4 us
    dot_general x2, matrix products, one_block(): jnp.einsum('kgqs,skd->qkgd', weights.astype(jnp.bfloat16), value_block, p...  9.75 us
    all_to_all x1, starting transfers between devices, body(): lax.all_to_all(summed.astype(jnp.bfloat16), 'ep', split_axis=0, concat_ax...  5.52 us
  transfers between devices with their start and end apart: 5, of which 4 were waited for; matrix products, arithmetic and copies ran while one was open for 12% of the time, Pallas kernels for 0%

profile of v1, /device:TPU:0, one launch (start us, length us, event | category | flops | bytes accessed | tf_op | source)
XLA Modules:
  0.0 268.9 jit_solution(5126965259523902607)
XLA Ops:
  7.2 0.9 copy.21
  10.1 1.2 fusion.42
  11.4 1.2 fusion.44
  13.3 1.2 reshape.297
  14.6 3.1 %scatter_custom_fusion = bf16[288,2048]{1,0:T(8,128)(2,1)S(1)} fusion(s32[256]{0:T(256)S(1)} %bitcast.139, bf16[256,2048]{1,0:T(8,128)(2,1)} %reshape.297, bf16[]{:T(256)} %constant.85.clone.1), kind=kCustom, calls=%fused_computation.50 | custom fusion | bytes 1180160 | tf_op jit(solution)/shard_map/scatter | solution.py:124
  18.0 38.5 %all_to_all.15 = bf16[8,36,2048]{2,1,0:T(8,128)(2,1)S(1)} all-to-all(bf16[8,36,2048]{2,1,0:T(8,128)(2,1)S(1)} %reshape.280), channel_id=1, replica_groups=mesh['ep'=8,'tp'=4] {'ep'}, dimensions={0} | all-to-all | bytes 2359296 | tf_op jit(solution)/shard_map/all_to_all | solution.py:129
  57.2 62.2 %all_to_all.16 = bf16[32,36,2048]{2,1,0:T(8,128)(2,1)S(1)} all-to-all(bf16[32,36,2048]{2,1,0:T(8,128)(2,1)S(1)} %bitcast.133), channel_id=1, replica_groups=mesh['ep'=8,'tp'=4] {'tp'}, dimensions={0} | all-to-all | bytes 9437184 | tf_op jit(solution)/shard_map/all_to_all | solution.py:14
  119.4 2.3 copy-done.2
  121.7 12.1 %fusion.28 = f32[32,36,1792]{2,1,0:T(8,128)} fusion(bf16[32,36,2048]{2,1,0:T(8,128)(2,1)S(1)} %all_to_all.16, bf16[1,2048,1792]{2,1,0:T(8,128)(2,1)S(1)} %bitcast.143), kind=kOutput, calls=%fused_computation.37 | convolution fusion | flops 8455716864 | bytes 20316160 | tf_op jit(solution)/shard_map/scd,df->scf/dot_general | solution.py:34
  133.8 30.9 %fusion.37 = bf16[32,36,2048]{2,1,0:T(8,128)(2,1)} fusion(bf16[1,1792,2048]{2,1,0:T(8,128)(2,1)} %param.25, f32[32,36,1792]{2,1,0:T(8,128)} %fusion.28, bf16[32,36,2048]{2,1,0:T(8,128)(2,1)} %copy-done.2, bf16[1,2048,1792]{2,1,0:T(8,128)(2,1)} %param.23), kind=kOutput, calls=%fused_computation.42 | convolution fusion | flops 16926179328 | bytes 32374784 | tf_op jit(solution)/shard_map/scf,fd->scd/dot_general | solution.py:134
  164.9 3.5 %collective-permute-start = (bf16[128,128]{0,1:T(8,128)(2,1)S(1)}, bf16[128,128]{0,1:T(8,128)(2,1)S(1)}, u32[]{:S(2)}, u32[]{:S(2)}) collective-permute-start(bf16[128,128]{0,1:T(8,128)(2,1)S(1)} %get-tuple-element.124), channel_id=1, source_target_pairs={{0,4},{4,8},{8,12},{12,16},{16,20},{20,24},{24,28},{1,5},{5,9},{9,... | collective-permute-start | bytes 98312 | tf_op jit(solution)/shard_map/ppermute | solution.py:24
  168.4 1.5 collective-permute-start.1
  170.0 4.2 %collective-permute-done.1 = bf16[128,128]{0,1:T(8,128)(2,1)S(1)} collective-permute-done((bf16[128,128]{0,1:T(8,128)(2,1)S(1)}, bf16[128,128]{0,1:T(8,128)(2,1)S(1)}, u32[]{:S(2)}, u32[]{:S(2)}) %collective-permute-start.1) | collective-permute-done | bytes 32800 | tf_op jit(solution)/shard_map/ppermute | solution.py:25
  174.3 25.5 %while.12 = (s32[]{:T(128)}, bf16[2,512,256]{2,1,0:T(8,128)(2,1)S(1)}, s32[2]{0:T(128)S(1)}, bf16[1280,128]{0,1:T(8,128)(2,1)S(1)}, s32[]{:T(128)}, /*index=5*/b...) while((s32[]{:T(128)}, ...), condition=%wide.region_3.4_spmd, body=%wide.region_0.3_spmd.sunk | while | flops 422191360 | bytes 48526672 | solution.py:83
  175.7 0.8 fusion.66
  176.6 1.2 fusion.67
  177.9 2.6 copy-done.1
  180.5 1.4 fusion.68
  182.0 5.2 %fusion.70 = bf16[512,1,4,64]{0,3,2,1:T(8,128)(2,1)S(1)} fusion(f32[768,512,4]{1,0,2:T(8,128)} %copy-done.1, f32[4,512]{1,0:T(4,128)S(1)} %broadcast_maximum_fusion.2, pred[512,768]{0,1:T(8,128)(4,1)S(1)} %fusion.66, f32[512,4]{0,1:T(4,128)S(1)} %fusion.69, bf16[1280,128]{0,1:T(8,128)(2,1)S(1)} %get-tuple-element.208, s32[]{:T(128)S(6)} %select_n.57, ...), kind=kOutput, calls=%fused_computation.15.clone.1 | convolution fusion | flops 207880192 | bytes 7061512 | tf_op jit(solution)/shard_map/while/body/eval_jaxpr/kgqs,skd->qkgd/dot_general | solution.py:74
  188.8 0.8 fusion.66
  189.7 1.2 fusion.67
  191.0 2.6 copy-done.1
  193.6 1.4 fusion.68
  195.1 4.5 %fusion.70 = bf16[512,1,4,64]{0,3,2,1:T(8,128)(2,1)S(1)} fusion(f32[768,512,4]{1,0,2:T(8,128)} %copy-done.1, f32[4,512]{1,0:T(4,128)S(1)} %broadcast_maximum_fusion.2, pred[512,768]{0,1:T(8,128)(4,1)S(1)} %fusion.66, f32[512,4]{0,1:T(4,128)S(1)} %fusion.69, bf16[1280,128]{0,1:T(8,128)(2,1)S(1)} %get-tuple-element.208, s32[]{:T(128)S(6)} %select_n.57, ...), kind=kOutput, calls=%fused_computation.15.clone.1 | convolution fusion | flops 207880192 | bytes 7061512 | tf_op jit(solution)/shard_map/while/body/eval_jaxpr/kgqs,skd->qkgd/dot_general | solution.py:74
  199.8 3.2 %convolution_convert_fusion = bf16[1024,2048]{1,0:T(8,128)(2,1)} fusion(bf16[1024,256]{1,0:T(8,128)(2,1)S(1)} %bitcast.135, bf16[256,2048]{1,0:T(8,128)(2,1)S(1)} %copy-done), kind=kOutput, calls=%fused_computation.43 | convolution fusion | flops 1075838976 | bytes 5767168 | tf_op jit(solution)/shard_map/dot_general | solution.py:103
  203.0 11.4 %reduce-scatter.5.cloned.1.call-done = bf16[8,36,2048]{2,1,0:T(8,128)(2,1)} async-done(((bf16[32,36,2048]{2,1,0:T(8,128)(2,1)}), bf16[8,36,2048]{2,1,0:T(8,128)(2,1)}) %reduce-scatter.5.cloned.1.call-update) | async-done | bytes 1179664 | tf_op jit(solution)/shard_map/reduce_scatter | solution.py:137
  214.4 5.5 %all-to-all-start.2 = ((bf16[8,36,2048]{2,1,0:T(8,128)(2,1)}), bf16[8,36,2048]{2,1,0:T(8,128)(2,1)}, u32[]{:S(2)}, u32[]{:S(2)}) async-start(bf16[8,36,2048]{2,1,0:T(8,128)(2,1)} %reduce-scatter.5.cloned.1.call-done), calls=%async_computation.4 | async-start | bytes 2621440 | tf_op jit(solution)/shard_map/all_to_all | solution.py:143
  220.0 31.2 %all-to-all-done.2 = bf16[8,36,2048]{2,1,0:T(8,128)(2,1)} async-done(((bf16[8,36,2048]{2,1,0:T(8,128)(2,1)}), bf16[8,36,2048]{2,1,0:T(8,128)(2,1)}, u32[]{:S(2)}, u32[]{:S(2)}) %all-to-all-start.2) | async-done | bytes 1179680 | tf_op jit(solution)/shard_map/all_to_all | solution.py:143
  251.2 1.4 reshape.284
  252.6 2.7 %gather_fusion = f32[256,2048]{1,0:T(8,128)} fusion(f32[288,2048]{1,0:T(8,128)S(1)} %reshape.284, s32[1024]{0:T(1024)S(1)} %pad_clamp_fusion), kind=kCustom, calls=%fused_computation | custom fusion | bytes 4195328 | tf_op jit(solution)/shard_map/gather | solution.py:147
  255.3 2.5 gather.6
  257.8 3.9 %multiply_reduce_fusion = bf16[128,2048]{1,0:T(8,128)(2,1)} fusion(f32[128,2,2048]{2,1,0:T(2,128)S(1)} %gather.6, f32[128,2]{1,0:T(8,128)S(1)} %copy.23), kind=kLoop, calls=%fused_computation.44 | loop fusion | flops 786432 | bytes 2622464 | tf_op jit(solution)/shard_map/reduce_sum | solution.py:148
  (70 shorter events, 6.7 us)
Async XLA Ops:
  7.2 192.6 %copy-start = (bf16[256,2048]{1,0:T(8,128)(2,1)S(1)}, bf16[256,2048]{1,0:T(8,128)(2,1)}, u32[]{:S(2)}) copy-start(bf16[256,2048]{1,0:T(8,128)(2,1)} %param.18) | copy-start | bytes 3145732
  7.2 207.2 %reduce-scatter.5.cloned.1.call-start = ((), (), s32[]{:S(2)}) async-start(), calls=%async_computation.6 | async-start | bytes 6553600 | tf_op jit(solution)/shard_map/reduce_scatter | solution.py:137
  56.5 65.2 %slice-start = ((s8[7340032]{0:T(1024)(128)(4,1)}), s8[4194304]{0:T(1024)(128)(4,1)S(1)}, s32[]{:S(2)}) async-start(s8[7340032]{0:T(1024)(128)(4,1)} %bitcast.142), calls=%async_computation.7 | async-start | bytes 8388608
  57.2 64.5 %slice-start.1 = ((s8[7340032]{0:T(1024)(128)(4,1)}), s8[3145728]{0:T(1024)(128)(4,1)S(1)}, s32[]{:S(2)}) async-start(s8[7340032]{0:T(1024)(128)(4,1)} %bitcast.142), calls=%async_computation.8 | async-start | bytes 6291456
  119.4 2.3 copy-start.2
  133.8 31.0 %copy-start.4 = (bf16[1024,64]{0,1:T(8,128)(2,1)S(1)}, bf16[1024,64]{0,1:T(8,128)(2,1)}, u32[]{:S(2)}) copy-start(bf16[1024,64]{0,1:T(8,128)(2,1)} %param.15) | copy-start | bytes 393220
  133.8 31.1 %copy-start.5 = (bf16[1024,64]{0,1:T(8,128)(2,1)S(1)}, bf16[1024,64]{0,1:T(8,128)(2,1)}, u32[]{:S(2)}) copy-start(bf16[1024,64]{0,1:T(8,128)(2,1)} %param.16) | copy-start | bytes 393220
  164.8 9.5 %copy-start.3 = (bf16[1024,256]{1,0:T(8,128)(2,1)S(1)}, bf16[1024,256]{1,0:T(8,128)(2,1)}, u32[]{:S(2)}) copy-start(bf16[1024,256]{1,0:T(8,128)(2,1)} %param.14) | copy-start | bytes 1572868
  164.8 9.5 %copy-start.6 = (f32[4]{0:T(128)S(1)}, f32[4]{0:T(128)}, u32[]{:S(2)}) copy-start(f32[4]{0:T(128)} %param.17) | copy-start | bytes 52
  164.8 97.3 %reduce-scatter.3.cloned.1.call-start = ((), (), s32[]{:S(2)}) async-start(), calls=%async_computation.5 | async-start | bytes 5242880 | tf_op jit(solution)/shard_map/reduce_scatter | solution.py:102
  164.9 5.0 %collective-permute-start = (bf16[128,128]{0,1:T(8,128)(2,1)S(1)}, bf16[128,128]{0,1:T(8,128)(2,1)S(1)}, u32[]{:S(2)}, u32[]{:S(2)}) collective-permute-start(bf16[128,128]{0,1:T(8,128)(2,1)S(1)} %get-tuple-element.124), channel_id=1, source_target_pairs={{0,4},{4,8},{8,12},{12,16},{16,20},{20,24},{24,28},{1,5},{5,9},{9,... | collective-permute-start | bytes 98312 | tf_op jit(solution)/shard_map/ppermute | solution.py:24
  168.4 5.8 %collective-permute-start.1 = (bf16[128,128]{0,1:T(8,128)(2,1)S(1)}, bf16[128,128]{0,1:T(8,128)(2,1)S(1)}, u32[]{:S(2)}, u32[]{:S(2)}) collective-permute-start(bf16[128,128]{0,1:T(8,128)(2,1)S(1)} %get-tuple-element.125), channel_id=1, source_target_pairs={{4,0},{8,4},{12,8},{16,12},{20,16},{24,20},{28,24},{5,1},{9,5},{13... | collective-permute-start | bytes 98312 | tf_op jit(solution)/shard_map/ppermute | solution.py:25
  177.8 2.7 copy-start.1
  190.9 2.7 copy-start.1
  199.8 20.1 %copy-start.7 = (f32[128,2]{0,1:T(2,128)S(1)}, f32[128,2]{0,1:T(2,128)}, u32[]{:S(2)}) copy-start(f32[128,2]{0,1:T(2,128)} %param.22) | copy-start | bytes 3076
  214.4 36.8 %all-to-all-start.2 = ((bf16[8,36,2048]{2,1,0:T(8,128)(2,1)}), bf16[8,36,2048]{2,1,0:T(8,128)(2,1)}, u32[]{:S(2)}, u32[]{:S(2)}) async-start(bf16[8,36,2048]{2,1,0:T(8,128)(2,1)} %reduce-scatter.5.cloned.1.call-done), calls=%async_computation.4 | async-start | bytes 2621440 | tf_op jit(solution)/shard_map/all_to_all | solution.py:143
Sparse Core Ops, SparseCore 0:
  164.9 49.4 reduce-scatter.4
  217.5 44.5 reduce-scatter.2
